TPU v7x, 32 devices: a whole 2x2x4 slice. The times are simulated.
32 devices in a mesh: fs: 4 (over z), tp: 4 (over y, x), rep: 2 (over core).
Axes of the slice: x: 2, y: 2, z: 4, core: 2. Of those that a mesh axis runs over, the one named last changes fastest.
Arguments:
- up_weight: float32 [2048, 8192], P('fs', ('tp', 'rep')), may hold values from -0.125 to 0.125
- up_momentum: float32 [2048, 8192], P('fs', ('tp', 'rep')), may hold values from -24 to 24
- up_grads: bfloat16 [2, 2048, 8192], P('rep', 'fs', 'tp'), may hold values from -2.09375 to 2.09375
- out_weight: float32 [2048, 2048], P('fs', ('tp', 'rep')), may hold values from -0.125 to 0.125
- out_momentum: float32 [2048, 2048], P('fs', ('tp', 'rep')), may hold values from -24 to 24
- out_grads: bfloat16 [2, 2048, 2048], P('rep', 'fs', 'tp'), may hold values from -2.09375 to 2.09375
Outputs:
- up_weight_new: float32 [2048, 8192], P('fs', ('tp', 'rep'))
- up_momentum_new: float32 [2048, 8192], P('fs', ('tp', 'rep'))
- up_direction: float32 [2048, 8192], P('fs', ('tp', 'rep'))
- out_weight_new: float32 [2048, 2048], P('fs', ('tp', 'rep'))
- out_momentum_new: float32 [2048, 2048], P('fs', ('tp', 'rep'))
- out_direction: float32 [2048, 2048], P('fs', ('tp', 'rep'))
All inputs are finite; a program needn't handle non-finite values.
Results may differ from a plain program's by a relative error of at most 0.039.
Values may be sent and summed in bfloat16 or wider, within the bound.
No kernel may reach another device: no remote copies, remote signals or barrier semaphores. Data moves between devices by JAX's collectives and lax.ppermute only.
A program may use at most 64 MiB of HBM per device.

v0:
```python
import math
import jax
import jax.numpy as jnp
from jax import lax
from jax.sharding import PartitionSpec as P

ITERS = 3
MOMENT = 0.9
RATE = 0.02
COEF_A = 3.4445
COEF_B = -4.775
COEF_C = 2.0315


def local_gram(values, columns):
    return lax.dot_general(
        values, columns, (((1,), (1,)), ((), ())), preferred_element_type=jnp.float32
    )


def contract(gram, values, gram_axis):
    return lax.dot_general(
        gram, values, (((gram_axis,), (0,)), ((), ())), preferred_element_type=jnp.float32
    )


def second_product(gram, first_half, gram_axis):
    return contract(gram, lax.all_gather(first_half, "fs", axis=0, tiled=True), gram_axis)


def on_device(up_weight, up_momentum, up_grads, out_weight, out_momentum, out_grads):
    grad_up, grad_out = (
        lax.psum_scatter(
            up_grads[0].astype(jnp.float32).astype(jnp.bfloat16),
            "rep",
            scatter_dimension=1,
            tiled=True,
        ).astype(jnp.float32),
        lax.psum_scatter(
            out_grads[0].astype(jnp.float32).astype(jnp.bfloat16),
            "rep",
            scatter_dimension=1,
            tiled=True,
        ).astype(jnp.float32),
    )
    moments = [MOMENT * up_momentum + grad_up, MOMENT * out_momentum + grad_out]
    group = lax.axis_size("tp") * lax.axis_size("rep")
    current = moments
    for iteration in range(ITERS):
        values = [entry.astype(jnp.bfloat16) for entry in current]
        columns = (
            lax.all_gather(values[0], "fs", axis=0, tiled=True),
            lax.all_gather(values[1], "fs", axis=0, tiled=True),
        )
        gram_sums = (
            lax.psum(local_gram(values[0], columns[0]).astype(jnp.bfloat16), ("tp", "rep")).astype(
                jnp.float32
            ),
            lax.psum(local_gram(values[1], columns[1]).astype(jnp.bfloat16), ("tp", "rep")).astype(
                jnp.float32
            ),
        )
        gram_axis = 1
        if iteration == 0:
            totals = lax.psum(
                (jnp.sum(gram_sums[0] * gram_sums[0]), jnp.sum(gram_sums[1] * gram_sums[1])), "fs"
            )
        if iteration == 0:
            squares = [1.0 / (jnp.sqrt(total) + 1.0) for total in totals]
            factors = [jnp.sqrt(square) for square in squares]
        else:
            squares = [1.0, 1.0]
            factors = [1.0, 1.0]
        halves = [(gram_sums[index] * squares[index]).astype(jnp.bfloat16) for index in range(2)]
        products = [
            factors[index] * contract(halves[index], columns[index], gram_axis)
            for index in range(2)
        ]
        seconds = [
            second_product(halves[index], products[index].astype(jnp.bfloat16), gram_axis)
            for index in range(2)
        ]
        current = [
            COEF_A * factors[index] * current[index]
            + COEF_B * products[index]
            + COEF_C * seconds[index]
            for index in range(2)
        ]
    widths = [up_weight.shape[1] * group, out_weight.shape[1] * group]
    directions = [current[index] * math.sqrt(widths[index]) for index in range(2)]
    return (
        up_weight - RATE * directions[0],
        moments[0],
        directions[0],
        out_weight - RATE * directions[1],
        moments[1],
        directions[1],
    )


def solution(mesh):
    return jax.shard_map(
        on_device,
        mesh=mesh,
        in_specs=(
            P("fs", ("tp", "rep")),
            P("fs", ("tp", "rep")),
            P("rep", "fs", "tp"),
            P("fs", ("tp", "rep")),
            P("fs", ("tp", "rep")),
            P("rep", "fs", "tp"),
        ),
        out_specs=(
            P("fs", ("tp", "rep")),
            P("fs", ("tp", "rep")),
            P("fs", ("tp", "rep")),
            P("fs", ("tp", "rep")),
            P("fs", ("tp", "rep")),
            P("fs", ("tp", "rep")),
        ),
        check_vma=False,
    )
```

profile of v0, /device:TPU:0, one launch (start us, length us, event | category | flops | bytes accessed | tf_op | source)
XLA Modules:
  0.0 994.7 jit_solution(5314064352922162735)
XLA Ops:
  7.2 0.7 reduce-scatter.5.cloned.1.call-update
  8.0 0.7 reduce-scatter.3.cloned.1.call-update
  8.7 12.2 %reduce-scatter.5.cloned.1.call-done = bf16[512,256]{1,0:T(8,128)(2,1)} async-done(((bf16[512,512]{1,0:T(8,128)(2,1)}), bf16[512,256]{1,0:T(8,128)(2,1)}) %reduce-scatter.5.cloned.1.call-update) | async-done | bytes 262160 | tf_op jit(solution)/shard_map/reduce_scatter | solution.py:39
  20.9 1.9 fusion.25
  22.9 11.0 %reduce-scatter.3.cloned.1.call-done = bf16[512,1024]{1,0:T(8,128)(2,1)} async-done(((bf16[512,2048]{1,0:T(8,128)(2,1)}), bf16[512,1024]{1,0:T(8,128)(2,1)}) %reduce-scatter.3.cloned.1.call-update) | async-done | bytes 1048592 | tf_op jit(solution)/shard_map/reduce_scatter | solution.py:33
  33.9 3.3 fusion.26
  37.3 0.0 all-reduce.12.cloned.1.call-start
  37.3 28.1 %all-gather.25.cloned.1.call-done = bf16[2048,256]{1,0:T(8,128)(2,1)} async-done(((bf16[512,256]{1,0:T(8,128)(2,1)}), bf16[2048,256]{1,0:T(8,128)(2,1)}) %all-gather.25.cloned.1.call-update) | async-done | bytes 1048592 | tf_op jit(solution)/shard_map/all_gather | solution.py:53
  65.4 3.3 convolution_convert_fusion.2
  68.7 78.9 %all-gather.13.cloned.1.call-done = bf16[2048,1024]{1,0:T(8,128)(2,1)} async-done(((bf16[512,1024]{1,0:T(8,128)(2,1)}), bf16[2048,1024]{1,0:T(8,128)(2,1)}) %all-gather.13.cloned.1.call-update) | async-done | bytes 4194320 | tf_op jit(solution)/shard_map/all_gather | solution.py:52
  147.5 5.9 convolution_convert_fusion.5
  153.5 79.4 %all-reduce.12.cloned.1.call-done = (bf16[512,2048]{1,0:T(8,128)(2,1)}, bf16[512,2048]{1,0:T(8,128)(2,1)}) async-done(((bf16[512,2048]{1,0:T(8,128)(2,1)}, bf16[512,2048]{1,0:T(8,128)(2,1)}), (bf16[512,2048]{1,0:T(8,128)(2,1)}, bf16[512,2048]{1,0:T(8,128)(2,1)})) %all-reduce.12.cloned.1.call-update) | async-done | bytes 4194320 | tf_op jit(solution)/shard_map/psum | solution.py:56
  232.9 4.0 fusion
  236.9 12.3 %all-reduce = (f32[]{:T(128)}, f32[]{:T(128)}) all-reduce(f32[]{:T(128)} %get-tuple-element.42, f32[]{:T(128)} %get-tuple-element.43), channel_id=1, replica_groups=mesh['fs'=4,'tp'=4,'rep'=2] {'fs'}, use_global_device_ids=true, to_apply=%region_3.0 | all-reduce | flops 2 | bytes 16 | tf_op jit(solution)/shard_map/psum | solution.py:65
  250.0 3.3 fusion.28
  254.2 6.3 multiply_convert_fusion
  260.5 0.0 all-gather.29.cloned.1.call-start
  260.6 18.3 %all-gather.27.cloned.1.call-done = bf16[2048,256]{1,0:T(8,128)(2,1)} async-done(((bf16[512,256]{1,0:T(8,128)(2,1)}), bf16[2048,256]{1,0:T(8,128)(2,1)}) %all-gather.27.cloned.1.call-update) | async-done | bytes 1048592 | tf_op jit(solution)/shard_map/all_gather | solution.py:28
  278.8 3.6 fusion.29
  282.5 78.6 %all-gather.15.cloned.1.call-done = bf16[2048,1024]{1,0:T(8,128)(2,1)} async-done(((bf16[512,1024]{1,0:T(8,128)(2,1)}), bf16[2048,1024]{1,0:T(8,128)(2,1)}) %all-gather.15.cloned.1.call-update) | async-done | bytes 4194320 | tf_op jit(solution)/shard_map/all_gather | solution.py:28
  361.1 7.6 fusion.27
  368.7 0.2 all-reduce.10.cloned.1.call-start
  369.0 20.8 %all-gather.29.cloned.1.call-done = bf16[2048,256]{1,0:T(8,128)(2,1)} async-done(((bf16[512,256]{1,0:T(8,128)(2,1)}), bf16[2048,256]{1,0:T(8,128)(2,1)}) %all-gather.29.cloned.1.call-update) | async-done | bytes 1048592 | tf_op jit(solution)/shard_map/all_gather | solution.py:53
  389.8 3.3 convolution_convert_fusion.1
  393.1 79.0 %all-gather.17.cloned.1.call-done = bf16[2048,1024]{1,0:T(8,128)(2,1)} async-done(((bf16[512,1024]{1,0:T(8,128)(2,1)}), bf16[2048,1024]{1,0:T(8,128)(2,1)}) %all-gather.17.cloned.1.call-update) | async-done | bytes 4194320 | tf_op jit(solution)/shard_map/all_gather | solution.py:52
  472.1 5.9 convolution_convert_fusion.4
  478.0 0.0 all-gather.31.cloned.1.call-start
  478.0 79.4 %all-reduce.10.cloned.1.call-done = (bf16[512,2048]{1,0:T(8,128)(2,1)}, bf16[512,2048]{1,0:T(8,128)(2,1)}) async-done(((bf16[512,2048]{1,0:T(8,128)(2,1)}, bf16[512,2048]{1,0:T(8,128)(2,1)}), (bf16[512,2048]{1,0:T(8,128)(2,1)}, bf16[512,2048]{1,0:T(8,128)(2,1)})) %all-reduce.10.cloned.1.call-update) | async-done | bytes 4194320 | tf_op jit(solution)/shard_map/psum | solution.py:56
  557.5 3.0 fusion.32
  560.5 0.0 all-gather.19.cloned.1.call-start
  560.6 6.9 fusion.30
  567.5 0.0 all-gather.33.cloned.1.call-start
  567.6 21.1 %all-gather.31.cloned.1.call-done = bf16[2048,256]{1,0:T(8,128)(2,1)} async-done(((bf16[512,256]{1,0:T(8,128)(2,1)}), bf16[2048,256]{1,0:T(8,128)(2,1)}) %all-gather.31.cloned.1.call-update) | async-done | bytes 1048592 | tf_op jit(solution)/shard_map/all_gather | solution.py:28
  588.7 2.8 fusion.33
  591.6 78.7 %all-gather.19.cloned.1.call-done = bf16[2048,1024]{1,0:T(8,128)(2,1)} async-done(((bf16[512,1024]{1,0:T(8,128)(2,1)}), bf16[2048,1024]{1,0:T(8,128)(2,1)}) %all-gather.19.cloned.1.call-update) | async-done | bytes 4194320 | tf_op jit(solution)/shard_map/all_gather | solution.py:28
  670.3 8.4 fusion.31
  678.7 20.2 %all-gather.33.cloned.1.call-done = bf16[2048,256]{1,0:T(8,128)(2,1)} async-done(((bf16[512,256]{1,0:T(8,128)(2,1)}), bf16[2048,256]{1,0:T(8,128)(2,1)}) %all-gather.33.cloned.1.call-update) | async-done | bytes 1048592 | tf_op jit(solution)/shard_map/all_gather | solution.py:53
  698.9 3.3 convolution_convert_fusion
  702.2 78.3 %all-gather.21.cloned.1.call-done = bf16[2048,1024]{1,0:T(8,128)(2,1)} async-done(((bf16[512,1024]{1,0:T(8,128)(2,1)}), bf16[2048,1024]{1,0:T(8,128)(2,1)}) %all-gather.21.cloned.1.call-update) | async-done | bytes 4194320 | tf_op jit(solution)/shard_map/all_gather | solution.py:52
  780.5 5.9 convolution_convert_fusion.3
  786.4 79.4 %all-reduce.8.cloned.1.call-done = (bf16[512,2048]{1,0:T(8,128)(2,1)}, bf16[512,2048]{1,0:T(8,128)(2,1)}) async-done(((bf16[512,2048]{1,0:T(8,128)(2,1)}, bf16[512,2048]{1,0:T(8,128)(2,1)}), (bf16[512,2048]{1,0:T(8,128)(2,1)}, bf16[512,2048]{1,0:T(8,128)(2,1)})) %all-reduce.8.cloned.1.call-update) | async-done | bytes 4194320 | tf_op jit(solution)/shard_map/psum | solution.py:56
  865.9 3.0 fusion.35
  868.9 0.3 all-gather.23.cloned.1.call-start
  869.2 7.0 fusion.34
  876.2 20.9 %all-gather.35.cloned.1.call-done = bf16[2048,256]{1,0:T(8,128)(2,1)} async-done(((bf16[512,256]{1,0:T(8,128)(2,1)}), bf16[2048,256]{1,0:T(8,128)(2,1)}) %all-gather.35.cloned.1.call-update) | async-done | bytes 1048592 | tf_op jit(solution)/shard_map/all_gather | solution.py:28
  897.1 3.1 broadcast_multiply_fusion.1
  900.2 78.5 %all-gather.23.cloned.1.call-done = bf16[2048,1024]{1,0:T(8,128)(2,1)} async-done(((bf16[512,1024]{1,0:T(8,128)(2,1)}), bf16[2048,1024]{1,0:T(8,128)(2,1)}) %all-gather.23.cloned.1.call-update) | async-done | bytes 4194320 | tf_op jit(solution)/shard_map/all_gather | solution.py:28
  978.7 9.5 broadcast_multiply_fusion
  (59 shorter events, 0.7 us)
Async XLA Ops:
  7.2 13.7 %copy-start.14 = (f32[512,256]{1,0:T(8,128)S(1)}, f32[512,256]{1,0:T(8,128)}, u32[]{:S(2)}) copy-start(f32[512,256]{1,0:T(8,128)} %param.10) | copy-start | bytes 1572868
  7.2 13.7 %reduce-scatter.5.cloned.1.call-start = ((), (), s32[]{:S(2)}) async-start(), calls=%async_computation.9 | async-start | bytes 786432 | tf_op jit(solution)/shard_map/reduce_scatter | solution.py:39
  7.9 26.0 %copy-start.7 = (f32[512,1024]{1,0:T(8,128)S(1)}, f32[512,1024]{1,0:T(8,128)}, u32[]{:S(2)}) copy-start(f32[512,1024]{1,0:T(8,128)} %param.7) | copy-start | bytes 6291460
  7.9 26.0 %reduce-scatter.3.cloned.1.call-start = ((), (), s32[]{:S(2)}) async-start(), calls=%async_computation.2 | async-start | bytes 3145728 | tf_op jit(solution)/shard_map/reduce_scatter | solution.py:33
  8.7 56.7 %all-gather.25.cloned.1.call-start = ((), (), s32[]{:S(2)}) async-start(), calls=%async_computation.10 | async-start | bytes 1310720 | tf_op jit(solution)/shard_map/all_gather | solution.py:53
  22.8 42.6 %copy-start.6 = (bf16[512,256]{1,0:T(8,128)(2,1)S(1)}, bf16[512,256]{1,0:T(8,128)(2,1)}, u32[]{:S(2)}) copy-start(bf16[512,256]{1,0:T(8,128)(2,1)} %get-tuple-element.14) | copy-start | bytes 786436
  22.8 124.7 %all-gather.13.cloned.1.call-start = ((), (), s32[]{:S(2)}) async-start(), calls=%async_computation.3 | async-start | bytes 5242880 | tf_op jit(solution)/shard_map/all_gather | solution.py:52
  37.2 110.3 %copy-start.4 = (bf16[512,1024]{1,0:T(8,128)(2,1)S(1)}, bf16[512,1024]{1,0:T(8,128)(2,1)}, u32[]{:S(2)}) copy-start(bf16[512,1024]{1,0:T(8,128)(2,1)} %get-tuple-element.16) | copy-start | bytes 3145732
  37.3 195.7 %all-reduce.12.cloned.1.call-start = ((), (), s32[]{:S(2)}) async-start(), calls=%async_computation.18 | async-start | bytes 8388608 | tf_op jit(solution)/shard_map/psum | solution.py:56
  153.4 125.4 %all-gather.27.cloned.1.call-start = ((), (), s32[]{:S(2)}) async-start(), calls=%async_computation.11 | async-start | bytes 1310720 | tf_op jit(solution)/shard_map/all_gather | solution.py:28
  232.9 17.1 %copy-start.10 = (bf16[2048,256]{1,0:T(8,128)(2,1)S(1)}, bf16[2048,256]{1,0:T(8,128)(2,1)}, u32[]{:S(2)}) copy-start(bf16[2048,256]{1,0:T(8,128)(2,1)} %all-gather.25.cloned.1.call-done) | copy-start | bytes 3145732
  250.0 4.2 copy-start.9
  253.4 107.8 %all-gather.15.cloned.1.call-start = ((), (), s32[]{:S(2)}) async-start(), calls=%async_computation.4 | async-start | bytes 5242880 | tf_op jit(solution)/shard_map/all_gather | solution.py:28
  254.2 24.7 %copy-start.15 = (f32[512,256]{1,0:T(8,128)S(1)}, f32[512,256]{1,0:T(8,128)}, u32[]{:S(2)}) copy-start(f32[512,256]{1,0:T(8,128)} %get-tuple-element.15) | copy-start | bytes 1572868
  254.2 24.6 %copy-start.16 = (f32[512,256]{1,0:T(8,128)S(1)}, f32[512,256]{1,0:T(8,128)}, u32[]{:S(2)}) copy-start(f32[512,256]{1,0:T(8,128)} %get-tuple-element.27) | copy-start | bytes 1572868
  260.5 129.3 %all-gather.29.cloned.1.call-start = ((), (), s32[]{:S(2)}) async-start(), calls=%async_computation.12 | async-start | bytes 1310720 | tf_op jit(solution)/shard_map/all_gather | solution.py:53
  278.8 82.3 %copy-start.8 = (f32[512,1024]{1,0:T(8,128)S(1)}, f32[512,1024]{1,0:T(8,128)}, u32[]{:S(2)}) copy-start(f32[512,1024]{1,0:T(8,128)} %get-tuple-element.17) | copy-start | bytes 6291460
  282.5 189.6 %all-gather.17.cloned.1.call-start = ((), (), s32[]{:S(2)}) async-start(), calls=%async_computation.5 | async-start | bytes 5242880 | tf_op jit(solution)/shard_map/all_gather | solution.py:52
  361.1 28.6 %copy-start.13 = (bf16[512,256]{1,0:T(8,128)(2,1)S(1)}, bf16[512,256]{1,0:T(8,128)(2,1)}, u32[]{:S(2)}) copy-start(bf16[512,256]{1,0:T(8,128)(2,1)} %get-tuple-element.28) | copy-start | bytes 786436
  368.7 103.4 %copy-start.11 = (bf16[512,1024]{1,0:T(8,128)(2,1)S(1)}, bf16[512,1024]{1,0:T(8,128)(2,1)}, u32[]{:S(2)}) copy-start(bf16[512,1024]{1,0:T(8,128)(2,1)} %get-tuple-element.24) | copy-start | bytes 3145732
  368.7 188.7 %all-reduce.10.cloned.1.call-start = ((), (), s32[]{:S(2)}) async-start(), calls=%async_computation.17 | async-start | bytes 8388608 | tf_op jit(solution)/shard_map/psum | solution.py:56
  477.9 79.5 %copy-start.2 = (bf16[2048,256]{1,0:T(8,128)(2,1)S(1)}, bf16[2048,256]{1,0:T(8,128)(2,1)}, u32[]{:S(2)}) copy-start(bf16[2048,256]{1,0:T(8,128)(2,1)} %all-gather.29.cloned.1.call-done) | copy-start | bytes 3145732
  478.0 110.7 %all-gather.31.cloned.1.call-start = ((), (), s32[]{:S(2)}) async-start(), calls=%async_computation.13 | async-start | bytes 1310720 | tf_op jit(solution)/shard_map/all_gather | solution.py:28
  560.5 109.8 %all-gather.19.cloned.1.call-start = ((), (), s32[]{:S(2)}) async-start(), calls=%async_computation.6 | async-start | bytes 5242880 | tf_op jit(solution)/shard_map/all_gather | solution.py:28
  560.5 28.2 %copy-start = (bf16[512,2048]{1,0:T(8,128)(2,1)S(1)}, bf16[512,2048]{1,0:T(8,128)(2,1)}, u32[]{:S(2)}) copy-start(bf16[512,2048]{1,0:T(8,128)(2,1)} %get-tuple-element.11) | copy-start | bytes 6291460
  567.5 131.4 %all-gather.33.cloned.1.call-start = ((), (), s32[]{:S(2)}) async-start(), calls=%async_computation.14 | async-start | bytes 1310720 | tf_op jit(solution)/shard_map/all_gather | solution.py:53
  591.5 189.0 %all-gather.21.cloned.1.call-start = ((), (), s32[]{:S(2)}) async-start(), calls=%async_computation.7 | async-start | bytes 5242880 | tf_op jit(solution)/shard_map/all_gather | solution.py:52
  670.3 28.6 %copy-start.5 = (bf16[512,256]{1,0:T(8,128)(2,1)S(1)}, bf16[512,256]{1,0:T(8,128)(2,1)}, u32[]{:S(2)}) copy-start(bf16[512,256]{1,0:T(8,128)(2,1)} %get-tuple-element.36) | copy-start | bytes 786436
  678.6 101.9 %copy-start.12 = (bf16[512,1024]{1,0:T(8,128)(2,1)S(1)}, bf16[512,1024]{1,0:T(8,128)(2,1)}, u32[]{:S(2)}) copy-start(bf16[512,1024]{1,0:T(8,128)(2,1)} %get-tuple-element.32) | copy-start | bytes 3145732
  678.6 187.2 %all-reduce.8.cloned.1.call-start = ((), (), s32[]{:S(2)}) async-start(), calls=%async_computation.16 | async-start | bytes 8388608 | tf_op jit(solution)/shard_map/psum | solution.py:56
  786.4 79.5 %copy-start.3 = (bf16[2048,256]{1,0:T(8,128)(2,1)S(1)}, bf16[2048,256]{1,0:T(8,128)(2,1)}, u32[]{:S(2)}) copy-start(bf16[2048,256]{1,0:T(8,128)(2,1)} %all-gather.33.cloned.1.call-done) | copy-start | bytes 3145732
  786.4 110.7 %all-gather.35.cloned.1.call-start = ((), (), s32[]{:S(2)}) async-start(), calls=%async_computation.15 | async-start | bytes 1310720 | tf_op jit(solution)/shard_map/all_gather | solution.py:28
  868.9 109.8 %all-gather.23.cloned.1.call-start = ((), (), s32[]{:S(2)}) async-start(), calls=%async_computation.8 | async-start | bytes 5242880 | tf_op jit(solution)/shard_map/all_gather | solution.py:28
  869.2 27.9 %copy-start.1 = (bf16[512,2048]{1,0:T(8,128)(2,1)S(1)}, bf16[512,2048]{1,0:T(8,128)(2,1)}, u32[]{:S(2)}) copy-start(bf16[512,2048]{1,0:T(8,128)(2,1)} %get-tuple-element.9) | copy-start | bytes 6291460
Sparse Core Ops, SparseCore 0:
  10.2 10.6 reduce-scatter.4
  23.1 10.7 reduce-scatter.2
  36.1 29.2 all-gather.24
  67.4 80.1 all-gather.12
  153.5 79.3 all-reduce.11
  253.5 25.3 all-gather.26
  281.0 80.1 all-gather.14
  363.3 26.4 all-gather.28
  391.9 80.1 all-gather.16
  478.1 79.3 all-reduce.9
  560.6 28.0 all-gather.30
  590.1 80.1 all-gather.18
  672.4 26.4 all-gather.32
  700.3 80.0 all-gather.20
  786.5 79.3 all-reduce.7
  869.0 28.0 all-gather.34
  898.5 80.1 all-gather.22
where the time goes:
time: 995 us
  waiting for transfers between devices  864 us (87%)
  matrix products  91.9 us (9%)
  between operations  15.6 us (2%)
  blocking collectives  12.3 us (1%)
    all_gather x6, waiting for transfers between devices, second_product(): lax.all_gather(first_half, 'fs', axis=0, tiled=True)  296 us
    psum x3, waiting for transfers between devices, on_device(): lax.psum(local_gram(values[0], columns[0]).astype(jnp.bfloat16), ('tp', '...  238 us
    all_gather x3, waiting for transfers between devices, on_device(): lax.all_gather(values[0], 'fs', axis=0, tiled=True)  236 us
    all_gather x3, waiting for transfers between devices, on_device(): lax.all_gather(values[1], 'fs', axis=0, tiled=True)  69.1 us
    dot_general x12, matrix products, contract(): lax.dot_general(gram, values, (((gram_axis,), (0,)), ((), ())), preferred...  64.4 us
    dot_general x6, matrix products, local_gram(): lax.dot_general(values, columns, (((1,), (1,)), ((), ())), preferred_elem...  27.5 us
  transfers between devices with their start and end apart: 17, of which 17 were waited for; matrix products, arithmetic and copies ran while one was open for 6% of the time, Pallas kernels for 0%

commit v1 on v0

--- a/solution.py
+++ b/solution.py
@@ -1,3 +1,4 @@
+import functools
 import math
 import jax
 import jax.numpy as jnp
@@ -10,6 +11,15 @@
 COEF_A = 3.4445
 COEF_B = -4.775
 COEF_C = 2.0315
+
+
+def _obtain_plane(array_here, axis_key, mesh_dim):
+    for no in (axis_key, mesh_dim):
+        array_here = lax.psum(array_here, no)
+    return array_here
+
+
+feed_routes_all_up = functools.partial(_obtain_plane, axis_key="rep", mesh_dim="tp")
 
 
 def local_gram(values, columns):
@@ -53,7 +63,7 @@
             lax.all_gather(values[1], "fs", axis=0, tiled=True),
         )
         gram_sums = (
-            lax.psum(local_gram(values[0], columns[0]).astype(jnp.bfloat16), ("tp", "rep")).astype(
+            feed_routes_all_up(local_gram(values[0], columns[0]).astype(jnp.bfloat16)).astype(
                 jnp.float32
             ),
             lax.psum(local_gram(values[1], columns[1]).astype(jnp.bfloat16), ("tp", "rep")).astype(

time: 995 us -> 1230 us (1.24)
  waiting for transfers between devices: 864 us -> 1090 us
    psum x3 -> x9, waiting for transfers between devices: 238 us -> 457 us  [the longest x6 267 us: _obtain_plane(): array_here = lax.psum(array_here, no)]
  transfers between devices with their start and end apart: 17 -> 23, of which waited for: 17 -> 23; matrix products, arithmetic and copies ran while one was open for 6% -> 6% of each run, Pallas kernels for 0% -> 0%
where the time goes in v1:
time: 1230 us
  waiting for transfers between devices  1090 us (89%)
  matrix products  92.2 us (7%)
  between operations  15.7 us (1%)
  blocking collectives  12.3 us (1%)
    all_gather x6, waiting for transfers between devices, second_product(): lax.all_gather(first_half, 'fs', axis=0, tiled=True)  301 us
    psum x6, waiting for transfers between devices, _obtain_plane(): array_here = lax.psum(array_here, no)  267 us
    all_gather x3, waiting for transfers between devices, on_device(): lax.all_gather(values[0], 'fs', axis=0, tiled=True)  236 us
    psum x3, waiting for transfers between devices, on_device(): lax.psum(local_gram(values[1], columns[1]).astype(jnp.bfloat16), ('tp', '...  190 us
    all_gather x3, waiting for transfers between devices, on_device(): lax.all_gather(values[1], 'fs', axis=0, tiled=True)  75.9 us
    dot_general x12, matrix products, contract(): lax.dot_general(gram, values, (((gram_axis,), (0,)), ((), ())), preferred...  64.1 us
    dot_general x6, matrix products, local_gram(): lax.dot_general(values, columns, (((1,), (1,)), ((), ())), preferred_elem...  28.1 us
  transfers between devices with their start and end apart: 23, of which 23 were waited for; matrix products, arithmetic and copies ran while one was open for 6% of the time, Pallas kernels for 0%

profile of v1, /device:TPU:0, one launch (start us, length us, event | category | flops | bytes accessed | tf_op | source)
XLA Modules:
  0.0 1226.3 jit_solution(3173638346339867813)
XLA Ops:
  7.2 0.7 reduce-scatter.3.cloned.1.call-update
  8.0 0.7 reduce-scatter.5.cloned.1.call-update
  8.7 13.9 %reduce-scatter.3.cloned.1.call-done = bf16[512,1024]{1,0:T(8,128)(2,1)} async-done(((bf16[512,2048]{1,0:T(8,128)(2,1)}), bf16[512,1024]{1,0:T(8,128)(2,1)}) %reduce-scatter.3.cloned.1.call-update) | async-done | bytes 1048592 | tf_op jit(solution)/shard_map/reduce_scatter | solution.py:43
  22.6 3.3 fusion.26
  26.0 8.1 reduce-scatter.5.cloned.1.call-done
  34.1 1.9 fusion.25
  36.1 82.1 %all-gather.13.cloned.1.call-done = bf16[2048,1024]{1,0:T(8,128)(2,1)} async-done(((bf16[512,1024]{1,0:T(8,128)(2,1)}), bf16[2048,1024]{1,0:T(8,128)(2,1)}) %all-gather.13.cloned.1.call-update) | async-done | bytes 4194320 | tf_op jit(solution)/shard_map/all_gather | solution.py:62
  118.1 5.9 convolution_convert_fusion.5
  124.1 22.5 %all-gather.25.cloned.1.call-done = bf16[2048,256]{1,0:T(8,128)(2,1)} async-done(((bf16[512,256]{1,0:T(8,128)(2,1)}), bf16[2048,256]{1,0:T(8,128)(2,1)}) %all-gather.25.cloned.1.call-update) | async-done | bytes 1048592 | tf_op jit(solution)/shard_map/all_gather | solution.py:63
  146.6 3.3 convolution_convert_fusion.2
  150.0 20.1 %all-reduce.11.cloned.1.call-done = bf16[512,2048]{1,0:T(8,128)(2,1)} async-done(((bf16[512,2048]{1,0:T(8,128)(2,1)}), bf16[512,2048]{1,0:T(8,128)(2,1)}) %all-reduce.11.cloned.1.call-update) | async-done | bytes 2097168 | tf_op jit(solution)/shard_map/psum | solution.py:18
  170.2 66.6 %all-reduce.23.cloned.1.call-done = bf16[512,2048]{1,0:T(8,128)(2,1)} async-done(((bf16[512,2048]{1,0:T(8,128)(2,1)}), bf16[512,2048]{1,0:T(8,128)(2,1)}) %all-reduce.23.cloned.1.call-update) | async-done | bytes 2097168 | tf_op jit(solution)/shard_map/psum | solution.py:69
  236.8 3.3 fusion.2
  240.0 68.4 %all-reduce.13.cloned.1.call-done = bf16[512,2048]{1,0:T(8,128)(2,1)} async-done(((bf16[512,2048]{1,0:T(8,128)(2,1)}), bf16[512,2048]{1,0:T(8,128)(2,1)}) %all-reduce.13.cloned.1.call-update) | async-done | bytes 2097168 | tf_op jit(solution)/shard_map/psum | solution.py:18
  308.4 3.3 fusion
  311.7 12.3 %all-reduce = (f32[]{:T(128)}, f32[]{:T(128)}) all-reduce(f32[]{:T(128)} %fusion, f32[]{:T(128)} %fusion.2), channel_id=1, replica_groups=mesh['fs'=4,'tp'=4,'rep'=2] {'fs'}, use_global_device_ids=true, to_apply=%region_4.0 | all-reduce | flops 2 | bytes 16 | tf_op jit(solution)/shard_map/psum | solution.py:75
  324.8 7.0 multiply_convert_fusion
  331.8 78.1 %all-gather.15.cloned.1.call-done = bf16[2048,1024]{1,0:T(8,128)(2,1)} async-done(((bf16[512,1024]{1,0:T(8,128)(2,1)}), bf16[2048,1024]{1,0:T(8,128)(2,1)}) %all-gather.15.cloned.1.call-update) | async-done | bytes 4194320 | tf_op jit(solution)/shard_map/all_gather | solution.py:38
  409.9 7.6 fusion.27
  418.4 3.3 fusion.31
  421.9 75.0 %all-gather.17.cloned.1.call-done = bf16[2048,1024]{1,0:T(8,128)(2,1)} async-done(((bf16[512,1024]{1,0:T(8,128)(2,1)}), bf16[2048,1024]{1,0:T(8,128)(2,1)}) %all-gather.17.cloned.1.call-update) | async-done | bytes 4194320 | tf_op jit(solution)/shard_map/all_gather | solution.py:62
  497.0 6.0 convolution_convert_fusion.4
  503.0 22.4 %all-gather.27.cloned.1.call-done = bf16[2048,256]{1,0:T(8,128)(2,1)} async-done(((bf16[512,256]{1,0:T(8,128)(2,1)}), bf16[2048,256]{1,0:T(8,128)(2,1)}) %all-gather.27.cloned.1.call-update) | async-done | bytes 1048592 | tf_op jit(solution)/shard_map/all_gather | solution.py:38
  525.5 2.8 fusion.32
  528.4 20.7 %all-reduce.15.cloned.1.call-done = bf16[512,2048]{1,0:T(8,128)(2,1)} async-done(((bf16[512,2048]{1,0:T(8,128)(2,1)}), bf16[512,2048]{1,0:T(8,128)(2,1)}) %all-reduce.15.cloned.1.call-update) | async-done | bytes 2097168 | tf_op jit(solution)/shard_map/psum | solution.py:18
  549.2 31.1 %all-gather.29.cloned.1.call-done = bf16[2048,256]{1,0:T(8,128)(2,1)} async-done(((bf16[512,256]{1,0:T(8,128)(2,1)}), bf16[2048,256]{1,0:T(8,128)(2,1)}) %all-gather.29.cloned.1.call-update) | async-done | bytes 1048592 | tf_op jit(solution)/shard_map/all_gather | solution.py:63
  580.3 3.4 convolution_convert_fusion.1
  583.8 68.5 %all-reduce.17.cloned.1.call-done = bf16[512,2048]{1,0:T(8,128)(2,1)} async-done(((bf16[512,2048]{1,0:T(8,128)(2,1)}), bf16[512,2048]{1,0:T(8,128)(2,1)}) %all-reduce.17.cloned.1.call-update) | async-done | bytes 2097168 | tf_op jit(solution)/shard_map/psum | solution.py:18
  652.3 6.8 fusion.28
  659.2 58.0 %all-reduce.25.cloned.1.call-done = bf16[512,2048]{1,0:T(8,128)(2,1)} async-done(((bf16[512,2048]{1,0:T(8,128)(2,1)}), bf16[512,2048]{1,0:T(8,128)(2,1)}) %all-reduce.25.cloned.1.call-update) | async-done | bytes 2097168 | tf_op jit(solution)/shard_map/psum | solution.py:69
  717.2 3.0 fusion.33
  720.3 78.2 %all-gather.19.cloned.1.call-done = bf16[2048,1024]{1,0:T(8,128)(2,1)} async-done(((bf16[512,1024]{1,0:T(8,128)(2,1)}), bf16[2048,1024]{1,0:T(8,128)(2,1)}) %all-gather.19.cloned.1.call-update) | async-done | bytes 4194320 | tf_op jit(solution)/shard_map/all_gather | solution.py:38
  798.5 8.4 fusion.29
  807.0 20.0 %all-gather.31.cloned.1.call-done = bf16[2048,256]{1,0:T(8,128)(2,1)} async-done(((bf16[512,256]{1,0:T(8,128)(2,1)}), bf16[2048,256]{1,0:T(8,128)(2,1)}) %all-gather.31.cloned.1.call-update) | async-done | bytes 1048592 | tf_op jit(solution)/shard_map/all_gather | solution.py:38
  827.0 2.8 fusion.34
  829.8 78.7 %all-gather.21.cloned.1.call-done = bf16[2048,1024]{1,0:T(8,128)(2,1)} async-done(((bf16[512,1024]{1,0:T(8,128)(2,1)}), bf16[2048,1024]{1,0:T(8,128)(2,1)}) %all-gather.21.cloned.1.call-update) | async-done | bytes 4194320 | tf_op jit(solution)/shard_map/all_gather | solution.py:62
  908.5 6.2 convolution_convert_fusion.3
  914.8 22.2 %all-gather.33.cloned.1.call-done = bf16[2048,256]{1,0:T(8,128)(2,1)} async-done(((bf16[512,256]{1,0:T(8,128)(2,1)}), bf16[2048,256]{1,0:T(8,128)(2,1)}) %all-gather.33.cloned.1.call-update) | async-done | bytes 1048592 | tf_op jit(solution)/shard_map/all_gather | solution.py:63
  937.0 3.4 convolution_convert_fusion
  940.5 20.2 %all-reduce.19.cloned.1.call-done = bf16[512,2048]{1,0:T(8,128)(2,1)} async-done(((bf16[512,2048]{1,0:T(8,128)(2,1)}), bf16[512,2048]{1,0:T(8,128)(2,1)}) %all-reduce.19.cloned.1.call-update) | async-done | bytes 2097168 | tf_op jit(solution)/shard_map/psum | solution.py:18
  960.9 65.8 %all-reduce.27.cloned.1.call-done = bf16[512,2048]{1,0:T(8,128)(2,1)} async-done(((bf16[512,2048]{1,0:T(8,128)(2,1)}), bf16[512,2048]{1,0:T(8,128)(2,1)}) %all-reduce.27.cloned.1.call-update) | async-done | bytes 2097168 | tf_op jit(solution)/shard_map/psum | solution.py:69
  1026.7 3.0 fusion.35
  1029.8 68.6 %all-reduce.21.cloned.1.call-done = bf16[512,2048]{1,0:T(8,128)(2,1)} async-done(((bf16[512,2048]{1,0:T(8,128)(2,1)}), bf16[512,2048]{1,0:T(8,128)(2,1)}) %all-reduce.21.cloned.1.call-update) | async-done | bytes 2097168 | tf_op jit(solution)/shard_map/psum | solution.py:18
  1098.4 6.8 fusion.30
  1105.2 23.3 %all-gather.35.cloned.1.call-done = bf16[2048,256]{1,0:T(8,128)(2,1)} async-done(((bf16[512,256]{1,0:T(8,128)(2,1)}), bf16[2048,256]{1,0:T(8,128)(2,1)}) %all-gather.35.cloned.1.call-update) | async-done | bytes 1048592 | tf_op jit(solution)/shard_map/all_gather | solution.py:38
  1128.6 3.1 broadcast_multiply_fusion.1
  1131.6 78.6 %all-gather.23.cloned.1.call-done = bf16[2048,1024]{1,0:T(8,128)(2,1)} async-done(((bf16[512,1024]{1,0:T(8,128)(2,1)}), bf16[2048,1024]{1,0:T(8,128)(2,1)}) %all-gather.23.cloned.1.call-update) | async-done | bytes 4194320 | tf_op jit(solution)/shard_map/all_gather | solution.py:38
  1210.3 9.5 broadcast_multiply_fusion
  (76 shorter events, 1.7 us)
Async XLA Ops:
  7.2 15.4 %copy-start.7 = (f32[512,1024]{1,0:T(8,128)S(1)}, f32[512,1024]{1,0:T(8,128)}, u32[]{:S(2)}) copy-start(f32[512,1024]{1,0:T(8,128)} %param.7) | copy-start | bytes 6291460
  7.2 15.4 %reduce-scatter.3.cloned.1.call-start = ((), (), s32[]{:S(2)}) async-start(), calls=%async_computation.2 | async-start | bytes 3145728 | tf_op jit(solution)/shard_map/reduce_scatter | solution.py:43
  7.9 26.2 %reduce-scatter.5.cloned.1.call-start = ((), (), s32[]{:S(2)}) async-start(), calls=%async_computation.15 | async-start | bytes 786432 | tf_op jit(solution)/shard_map/reduce_scatter | solution.py:49
  8.7 25.4 %copy-start.13 = (f32[512,256]{1,0:T(8,128)S(1)}, f32[512,256]{1,0:T(8,128)}, u32[]{:S(2)}) copy-start(f32[512,256]{1,0:T(8,128)} %param.10) | copy-start | bytes 1572868
  8.7 109.5 %all-gather.13.cloned.1.call-start = ((), (), s32[]{:S(2)}) async-start(), calls=%async_computation.3 | async-start | bytes 5242880 | tf_op jit(solution)/shard_map/all_gather | solution.py:62
  25.9 92.2 %copy-start.4 = (bf16[512,1024]{1,0:T(8,128)(2,1)S(1)}, bf16[512,1024]{1,0:T(8,128)(2,1)}, u32[]{:S(2)}) copy-start(bf16[512,1024]{1,0:T(8,128)(2,1)} %get-tuple-element.10) | copy-start | bytes 3145732
  25.9 120.7 %all-gather.25.cloned.1.call-start = ((), (), s32[]{:S(2)}) async-start(), calls=%async_computation.16 | async-start | bytes 1310720 | tf_op jit(solution)/shard_map/all_gather | solution.py:63
  36.0 134.1 %all-reduce.11.cloned.1.call-start = ((), (), s32[]{:S(2)}) async-start(), calls=%async_computation.4 | async-start | bytes 4194304 | tf_op jit(solution)/shard_map/psum | solution.py:18
  124.0 22.6 %copy-start.6 = (bf16[512,256]{1,0:T(8,128)(2,1)S(1)}, bf16[512,256]{1,0:T(8,128)(2,1)}, u32[]{:S(2)}) copy-start(bf16[512,256]{1,0:T(8,128)(2,1)} %get-tuple-element.8) | copy-start | bytes 786436
  124.0 112.7 %all-reduce.23.cloned.1.call-start = ((), (), s32[]{:S(2)}) async-start(), calls=%async_computation.17 | async-start | bytes 4194304 | tf_op jit(solution)/shard_map/psum | solution.py:69
  149.9 158.5 %all-reduce.13.cloned.1.call-start = ((), (), s32[]{:S(2)}) async-start(), calls=%async_computation.5 | async-start | bytes 4194304 | tf_op jit(solution)/shard_map/psum | solution.py:18
  170.1 239.8 %all-gather.15.cloned.1.call-start = ((), (), s32[]{:S(2)}) async-start(), calls=%async_computation.6 | async-start | bytes 5242880 | tf_op jit(solution)/shard_map/all_gather | solution.py:38
  324.8 85.1 %copy-start.8 = (f32[512,1024]{1,0:T(8,128)S(1)}, f32[512,1024]{1,0:T(8,128)}, u32[]{:S(2)}) copy-start(f32[512,1024]{1,0:T(8,128)} %get-tuple-element.11) | copy-start | bytes 6291460
  331.8 165.2 %all-gather.17.cloned.1.call-start = ((), (), s32[]{:S(2)}) async-start(), calls=%async_computation.7 | async-start | bytes 5242880 | tf_op jit(solution)/shard_map/all_gather | solution.py:62
  409.9 8.5 copy-start.10
  417.6 107.9 %all-gather.27.cloned.1.call-start = ((), (), s32[]{:S(2)}) async-start(), calls=%async_computation.18 | async-start | bytes 1310720 | tf_op jit(solution)/shard_map/all_gather | solution.py:38
  418.4 78.6 %copy-start.11 = (bf16[512,1024]{1,0:T(8,128)(2,1)S(1)}, bf16[512,1024]{1,0:T(8,128)(2,1)}, u32[]{:S(2)}) copy-start(bf16[512,1024]{1,0:T(8,128)(2,1)} %get-tuple-element.18) | copy-start | bytes 3145732
  421.7 127.4 %all-reduce.15.cloned.1.call-start = ((), (), s32[]{:S(2)}) async-start(), calls=%async_computation.8 | async-start | bytes 4194304 | tf_op jit(solution)/shard_map/psum | solution.py:18
  496.9 28.5 %copy-start.14 = (f32[512,256]{1,0:T(8,128)S(1)}, f32[512,256]{1,0:T(8,128)}, u32[]{:S(2)}) copy-start(f32[512,256]{1,0:T(8,128)} %get-tuple-element.9) | copy-start | bytes 1572868
  497.0 28.5 %copy-start.15 = (f32[512,256]{1,0:T(8,128)S(1)}, f32[512,256]{1,0:T(8,128)}, u32[]{:S(2)}) copy-start(f32[512,256]{1,0:T(8,128)} %get-tuple-element.27) | copy-start | bytes 1572868
  502.9 22.5 %copy-start.9 = (bf16[512,2048]{1,0:T(8,128)(2,1)S(1)}, bf16[512,2048]{1,0:T(8,128)(2,1)}, u32[]{:S(2)}) copy-start(bf16[512,2048]{1,0:T(8,128)(2,1)} %all-reduce.23.cloned.1.call-done) | copy-start | bytes 6291460
  502.9 77.3 %all-gather.29.cloned.1.call-start = ((), (), s32[]{:S(2)}) async-start(), calls=%async_computation.19 | async-start | bytes 1310720 | tf_op jit(solution)/shard_map/all_gather | solution.py:63
  528.3 52.0 %copy-start.12 = (bf16[512,256]{1,0:T(8,128)(2,1)S(1)}, bf16[512,256]{1,0:T(8,128)(2,1)}, u32[]{:S(2)}) copy-start(bf16[512,256]{1,0:T(8,128)(2,1)} %get-tuple-element.28) | copy-start | bytes 786436
  528.3 124.0 %all-reduce.17.cloned.1.call-start = ((), (), s32[]{:S(2)}) async-start(), calls=%async_computation.9 | async-start | bytes 4194304 | tf_op jit(solution)/shard_map/psum | solution.py:18
  549.1 168.1 %all-reduce.25.cloned.1.call-start = ((), (), s32[]{:S(2)}) async-start(), calls=%async_computation.20 | async-start | bytes 4194304 | tf_op jit(solution)/shard_map/psum | solution.py:69
  583.7 133.5 %copy-start.2 = (bf16[2048,256]{1,0:T(8,128)(2,1)S(1)}, bf16[2048,256]{1,0:T(8,128)(2,1)}, u32[]{:S(2)}) copy-start(bf16[2048,256]{1,0:T(8,128)(2,1)} %all-gather.29.cloned.1.call-done) | copy-start | bytes 3145732
  583.7 214.7 %all-gather.19.cloned.1.call-start = ((), (), s32[]{:S(2)}) async-start(), calls=%async_computation.10 | async-start | bytes 5242880 | tf_op jit(solution)/shard_map/all_gather | solution.py:38
  659.1 167.8 %all-gather.31.cloned.1.call-start = ((), (), s32[]{:S(2)}) async-start(), calls=%async_computation.21 | async-start | bytes 1310720 | tf_op jit(solution)/shard_map/all_gather | solution.py:38
  720.2 188.3 %all-gather.21.cloned.1.call-start = ((), (), s32[]{:S(2)}) async-start(), calls=%async_computation.11 | async-start | bytes 5242880 | tf_op jit(solution)/shard_map/all_gather | solution.py:62
  798.4 28.5 %copy-start = (bf16[512,2048]{1,0:T(8,128)(2,1)S(1)}, bf16[512,2048]{1,0:T(8,128)(2,1)}, u32[]{:S(2)}) copy-start(bf16[512,2048]{1,0:T(8,128)(2,1)} %all-reduce.25.cloned.1.call-done) | copy-start | bytes 6291460
  806.9 130.1 %all-gather.33.cloned.1.call-start = ((), (), s32[]{:S(2)}) async-start(), calls=%async_computation.22 | async-start | bytes 1310720 | tf_op jit(solution)/shard_map/all_gather | solution.py:63
  829.8 130.9 %all-reduce.19.cloned.1.call-start = ((), (), s32[]{:S(2)}) async-start(), calls=%async_computation.12 | async-start | bytes 4194304 | tf_op jit(solution)/shard_map/psum | solution.py:18
  914.7 22.3 %copy-start.5 = (bf16[512,256]{1,0:T(8,128)(2,1)S(1)}, bf16[512,256]{1,0:T(8,128)(2,1)}, u32[]{:S(2)}) copy-start(bf16[512,256]{1,0:T(8,128)(2,1)} %get-tuple-element.32) | copy-start | bytes 786436
  914.7 112.0 %all-reduce.27.cloned.1.call-start = ((), (), s32[]{:S(2)}) async-start(), calls=%async_computation.23 | async-start | bytes 4194304 | tf_op jit(solution)/shard_map/psum | solution.py:69
  940.4 86.3 %copy-start.3 = (bf16[2048,256]{1,0:T(8,128)(2,1)S(1)}, bf16[2048,256]{1,0:T(8,128)(2,1)}, u32[]{:S(2)}) copy-start(bf16[2048,256]{1,0:T(8,128)(2,1)} %all-gather.33.cloned.1.call-done) | copy-start | bytes 3145732
  940.4 158.0 %all-reduce.21.cloned.1.call-start = ((), (), s32[]{:S(2)}) async-start(), calls=%async_computation.13 | async-start | bytes 4194304 | tf_op jit(solution)/shard_map/psum | solution.py:18
  960.7 167.9 %all-gather.35.cloned.1.call-start = ((), (), s32[]{:S(2)}) async-start(), calls=%async_computation.24 | async-start | bytes 1310720 | tf_op jit(solution)/shard_map/all_gather | solution.py:38
  1029.7 98.8 %copy-start.1 = (bf16[512,2048]{1,0:T(8,128)(2,1)S(1)}, bf16[512,2048]{1,0:T(8,128)(2,1)}, u32[]{:S(2)}) copy-start(bf16[512,2048]{1,0:T(8,128)(2,1)} %all-reduce.27.cloned.1.call-done) | copy-start | bytes 6291460
  1029.7 180.5 %all-gather.23.cloned.1.call-start = ((), (), s32[]{:S(2)}) async-start(), calls=%async_computation.14 | async-start | bytes 5242880 | tf_op jit(solution)/shard_map/all_gather | solution.py:38
Sparse Core Ops, SparseCore 0:
  10.2 12.3 reduce-scatter.2
  24.8 9.2 reduce-scatter.4
  36.2 81.8 all-gather.12
  120.1 26.4 all-gather.24
  149.4 20.6 all-reduce.10
  173.8 62.9 all-reduce.22
  239.8 68.5 all-reduce.12
  331.9 77.9 all-gather.14
  417.7 79.2 all-gather.16
  498.9 26.4 all-gather.26
  528.4 20.6 all-reduce.14
  551.1 29.1 all-gather.28
  583.4 68.8 all-reduce.16
  655.4 61.7 all-reduce.24
  718.6 79.8 all-gather.18
  800.4 26.4 all-gather.30
  828.4 80.1 all-gather.20
  910.5 26.4 all-gather.32
  939.9 20.6 all-reduce.18
  963.7 62.9 all-reduce.26
  1029.8 68.5 all-reduce.20
  1100.5 27.9 all-gather.34
  1130.1 80.1 all-gather.22
